TPU v7x, 32 devices: a whole 2x2x4 slice. The times are simulated.
32 devices in a mesh: grp: 2 (over y), sp: 4 (over z), tp: 4 (over x, core).
Axes of the slice: x: 2, y: 2, z: 4, core: 2. Of those that a mesh axis runs over, the one named last changes fastest.
Arguments:
- tokens: bfloat16 [4096, 2048], P(('grp', 'sp'), 'tp'), parts along dimension 0, may hold values from -140 to 140, as said below
- mix_gain: bfloat16 [2, 2048], replicated, may hold values from 0.099609375 to 1.8984375
- gate_weight: bfloat16 [2, 2048, 2048], P(None, 'sp', 'tp'), may hold values from -0.125 to 0.125
- mix_weight: bfloat16 [2, 2048, 2048], P(None, 'sp', 'tp'), may hold values from -0.125 to 0.125
- value_weight: bfloat16 [2, 2048, 2048], P(None, 'sp', 'tp'), may hold values from -0.125 to 0.125
- out_weight: bfloat16 [2, 2048, 2048], P(None, 'sp', 'tp'), may hold values from -0.125 to 0.125
- conv_taps: bfloat16 [2, 3, 2048], P(None, None, 'tp'), may hold values from -3.5 to 3.5
Outputs:
- result_stream: bfloat16 [4096, 2048], P(('grp', 'sp'), 'tp'), parts along dimension 0
There are 2 independent parts, one for each index of `grp`. A program takes and returns all parts, laid end to end along the dimension named above; an argument that names none is the same for every part. Nothing has to cross between parts.
Inputs may be any that keep to these rules, and one draw needn't show every extreme that they name: `tokens`: activations with feature scales of several sizes.
All inputs are finite; a program needn't handle non-finite values.
Results may differ from a plain program's by a relative error of at most 0.015.
Values may be sent and summed in bfloat16 or wider, within the bound.
A program may use at most 64 MiB of HBM per device.

v0:
```python
import jax
import jax.numpy as jnp
from jax import lax
from jax.sharding import PartitionSpec as P

EPS = 1e-06


def passed_along(x, axis, by):
    devices = lax.axis_size(axis)
    pairs = [(i, i + by) for i in range(devices) if 0 <= i + by < devices]
    return lax.ppermute(x, axis, pairs)


def normed_rows(rows, gain):
    wide_rows = rows.astype(jnp.float32)
    factor = lax.rsqrt(jnp.mean(wide_rows * wide_rows, axis=1, keepdims=True) + EPS)
    return (wide_rows * factor * gain.astype(jnp.float32)).astype(jnp.bfloat16)


def convolve(carried, before, tap_rows):
    padded = jnp.concatenate([before, carried], axis=0)
    row_count = carried.shape[0]
    result = jnp.zeros_like(carried)
    for tap_index in range(tap_rows.shape[0]):
        result = (
            result
            + tap_rows[tap_index].astype(jnp.float32) * padded[tap_index : tap_index + row_count]
        )
    return result


def shards(tokens, mix_gain, gate_weight, mix_weight, value_weight, out_weight, conv_taps):
    layer_count = gate_weight.shape[0]
    conv_reach = conv_taps.shape[1] - 1
    fringe_depth = 0
    stream = tokens
    gathered = (
        lax.all_gather(gate_weight, "sp", axis=1, tiled=True),
        lax.all_gather(mix_weight, "sp", axis=1, tiled=True),
        lax.all_gather(value_weight, "sp", axis=1, tiled=True),
        lax.all_gather(out_weight, "sp", axis=1, tiled=True),
    )
    for layer_index in range(layer_count):
        whole = lax.all_gather(stream, "tp", axis=1, tiled=True)
        normed = normed_rows(whole, mix_gain[layer_index])
        gate = jnp.dot(normed, gathered[0][layer_index], preferred_element_type=jnp.float32)
        inner = jnp.dot(normed, gathered[1][layer_index], preferred_element_type=jnp.float32)
        values = jnp.dot(normed, gathered[2][layer_index], preferred_element_type=jnp.float32)
        gate = gate.astype(jnp.bfloat16)
        inner = inner.astype(jnp.bfloat16)
        values = values.astype(jnp.bfloat16)
        carried = inner.astype(jnp.float32) * values.astype(jnp.float32)
        before = passed_along(carried[carried.shape[0] - conv_reach :], "sp", 1)
        conv = convolve(carried, before, conv_taps[layer_index])
        mixed = (gate.astype(jnp.float32) * conv).astype(jnp.bfloat16)
        mixed_all = lax.all_gather(mixed, "tp", axis=1, tiled=True)
        product = jnp.dot(mixed_all, gathered[3][layer_index], preferred_element_type=jnp.float32)
        stream = (stream.astype(jnp.float32) + product).astype(jnp.bfloat16)
    return stream


def solution(mesh):
    return jax.shard_map(
        shards,
        mesh=mesh,
        in_specs=(
            P(("grp", "sp"), "tp"),
            P(),
            P(None, "sp", "tp"),
            P(None, "sp", "tp"),
            P(None, "sp", "tp"),
            P(None, "sp", "tp"),
            P(None, None, "tp"),
        ),
        out_specs=P(("grp", "sp"), "tp"),
        check_vma=False,
    )
```

profile of v0, /device:TPU:0, one launch (start us, length us, event | category | flops | bytes accessed | tf_op | source)
XLA Modules:
  0.0 456.6 jit_solution(16903297331807922796)
XLA Ops:
  6.5 0.0 all-gather.9.cloned.1.call-start
  6.5 0.7 all-gather.9.cloned.1.call-update
  7.3 0.0 copy-start.4
  7.3 0.0 all-gather.15.cloned.1.call-start
  7.3 0.7 all-gather.15.cloned.1.call-update
  8.0 0.0 all-gather.13.cloned.1.call-start
  8.1 0.7 all-gather.13.cloned.1.call-update
  8.8 0.0 all-gather.11.cloned.1.call-start
  8.8 0.5 all-gather.11.cloned.1.call-update
  9.3 0.0 all-gather.19.cloned.1.call-start
  9.4 0.5 all-gather.19.cloned.1.call-update
  9.9 0.0 all-gather.17.cloned.1.call-start
  10.0 0.0 copy-done.4
  10.0 24.2 %all-gather.9.cloned.1.call-done = bf16[512,2048]{1,0:T(8,128)(2,1)} async-done(((bf16[512,512]{1,0:T(8,128)(2,1)}), bf16[512,2048]{1,0:T(8,128)(2,1)}) %all-gather.9.cloned.1.call-update) | async-done | bytes 2097168 | tf_op jit(solution)/shard_map/all_gather | solution.py:45
  34.2 0.0 copy-start
  34.2 2.2 fusion
  36.4 80.1 %all-gather.15.cloned.1.call-done = bf16[2,2048,512]{2,1,0:T(8,128)(2,1)} async-done(((bf16[2,512,512]{2,1,0:T(8,128)(2,1)}), bf16[2,2048,512]{2,1,0:T(8,128)(2,1)}) %all-gather.15.cloned.1.call-update) | async-done | bytes 4194320 | tf_op jit(solution)/shard_map/all_gather | solution.py:41
  116.6 0.0 copy-done
  116.6 2.9 fusion.22
  119.5 0.0 copy-start.5
  119.5 77.9 %all-gather.13.cloned.1.call-done = bf16[2,2048,512]{2,1,0:T(8,128)(2,1)} async-done(((bf16[2,512,512]{2,1,0:T(8,128)(2,1)}), bf16[2,2048,512]{2,1,0:T(8,128)(2,1)}) %all-gather.13.cloned.1.call-update) | async-done | bytes 4194320 | tf_op jit(solution)/shard_map/all_gather | solution.py:40
  197.4 2.9 fusion.20
  200.3 0.0 copy-start.6
  200.3 1.3 collective-permute-start
  201.6 0.0 copy-done.6
  201.6 0.0 copy-done.5
  201.7 76.4 %all-gather.11.cloned.1.call-done = bf16[2,2048,512]{2,1,0:T(8,128)(2,1)} async-done(((bf16[2,512,512]{2,1,0:T(8,128)(2,1)}), bf16[2,2048,512]{2,1,0:T(8,128)(2,1)}) %all-gather.11.cloned.1.call-update) | async-done | bytes 4194320 | tf_op jit(solution)/shard_map/all_gather | solution.py:39
  278.1 0.0 collective-permute-done
  278.1 0.0 copy-start.2
  278.1 4.9 %fusion.43 = bf16[512,512]{1,0:T(8,128)(2,1)} fusion(f32[2,512]{1,0:T(2,128)S(1)} %collective-permute-done, f32[512,512]{1,0:T(8,128)} %copy-done.6, f32[512]{0:T(512)S(1)} %bitcast.83, f32[512]{0:T(512)S(1)} %bitcast.84, f32[512]{0:T(512)S(1)} %bitcast.85, bf16[2,2048,512]{2,1,0:T(8,128)(2,1)} %all-gather.11.cloned.1.call-done, ...), kind=kOutput, calls=%fused_computation.59 | convolution fusion | flops 1080819712 | bytes 5787648 | tf_op jit(solution)/shard_map/dot_general | solution.py:47
  283.0 0.0 all-gather.17.cloned.1.call-update
  283.0 0.0 all-gather.21.cloned.1.call-start
  283.1 75.7 %all-gather.19.cloned.1.call-done = bf16[2,2048,512]{2,1,0:T(8,128)(2,1)} async-done(((bf16[2,512,512]{2,1,0:T(8,128)(2,1)}), bf16[2,2048,512]{2,1,0:T(8,128)(2,1)}) %all-gather.19.cloned.1.call-update) | async-done | bytes 4194320 | tf_op jit(solution)/shard_map/all_gather | solution.py:42
  358.7 22.5 %all-gather.17.cloned.1.call-done = bf16[512,2048]{1,0:T(8,128)(2,1)} async-done(((bf16[512,512]{1,0:T(8,128)(2,1)}), bf16[512,2048]{1,0:T(8,128)(2,1)}) %all-gather.17.cloned.1.call-update) | async-done | bytes 2097168 | tf_op jit(solution)/shard_map/all_gather | solution.py:57
  381.2 0.0 copy-done.2
  381.2 4.3 fusion.31
  385.5 0.0 all-gather.21.cloned.1.call-update
  385.5 0.0 all-gather.23.cloned.1.call-start
  385.6 22.7 %all-gather.21.cloned.1.call-done = bf16[512,2048]{1,0:T(8,128)(2,1)} async-done(((bf16[512,512]{1,0:T(8,128)(2,1)}), bf16[512,2048]{1,0:T(8,128)(2,1)}) %all-gather.21.cloned.1.call-update) | async-done | bytes 2097168 | tf_op jit(solution)/shard_map/all_gather | solution.py:45
  408.3 0.0 copy-start.1
  408.3 2.2 fusion.3
  410.5 0.0 copy-done.1
  410.5 0.0 copy-start.8
  410.5 3.0 fusion.29
  413.6 0.0 copy-done.8
  413.6 0.0 copy-start.7
  413.6 1.3 fusion.27
  414.9 3.4 collective-permute-start.1
  418.3 1.3 collective-permute-done.1
  419.6 0.0 copy-done.7
  419.6 0.0 copy-start.3
  419.7 2.3 fusion.37
  422.0 0.0 all-gather.23.cloned.1.call-update
  422.0 23.5 %all-gather.23.cloned.1.call-done = bf16[512,2048]{1,0:T(8,128)(2,1)} async-done(((bf16[512,512]{1,0:T(8,128)(2,1)}), bf16[512,2048]{1,0:T(8,128)(2,1)}) %all-gather.23.cloned.1.call-update) | async-done | bytes 2097168 | tf_op jit(solution)/shard_map/all_gather | solution.py:57
  445.5 0.0 copy-done.3
  445.5 4.3 fusion.30
  (6 shorter events, 0.1 us)
Async XLA Ops:
  6.5 27.7 %all-gather.9.cloned.1.call-start = ((), (), s32[]{:S(2)}) async-start(), calls=%async_computation | async-start | bytes 2621440 | tf_op jit(solution)/shard_map/all_gather | solution.py:45
  7.3 2.7 copy-start.4
  7.3 109.3 %all-gather.15.cloned.1.call-start = ((), (), s32[]{:S(2)}) async-start(), calls=%async_computation.3 | async-start | bytes 5242880 | tf_op jit(solution)/shard_map/all_gather | solution.py:41
  8.0 189.4 %all-gather.13.cloned.1.call-start = ((), (), s32[]{:S(2)}) async-start(), calls=%async_computation.2 | async-start | bytes 5242880 | tf_op jit(solution)/shard_map/all_gather | solution.py:40
  8.8 269.3 %all-gather.11.cloned.1.call-start = ((), (), s32[]{:S(2)}) async-start(), calls=%async_computation.1 | async-start | bytes 5242880 | tf_op jit(solution)/shard_map/all_gather | solution.py:39
  9.3 349.4 %all-gather.19.cloned.1.call-start = ((), (), s32[]{:S(2)}) async-start(), calls=%async_computation.5 | async-start | bytes 5242880 | tf_op jit(solution)/shard_map/all_gather | solution.py:42
  9.9 371.3 %all-gather.17.cloned.1.call-start = ((), (), s32[]{:S(2)}) async-start(), calls=%async_computation.4 | async-start | bytes 2621440 | tf_op jit(solution)/shard_map/all_gather | solution.py:57
  34.2 82.3 %copy-start = (bf16[512,2048]{1,0:T(8,128)(2,1)S(1)}, bf16[512,2048]{1,0:T(8,128)(2,1)}, u32[]{:S(2)}) copy-start(bf16[512,2048]{1,0:T(8,128)(2,1)} %all-gather.9.cloned.1.call-done) | copy-start | bytes 6291460
  119.5 82.2 %copy-start.5 = (bf16[2,3,512]{2,0,1:T(2,128)(2,1)S(1)}, bf16[2,3,512]{2,0,1:T(2,128)(2,1)}, u32[]{:S(2)}) copy-start(bf16[2,3,512]{2,0,1:T(2,128)(2,1)} %param.13) | copy-start | bytes 18436
  200.3 1.3 copy-start.6
  200.3 77.8 %collective-permute-start = (f32[2,512]{1,0:T(2,128)S(1)}, f32[2,512]{1,0:T(2,128)S(1)}, u32[]{:S(2)}, u32[]{:S(2)}) collective-permute-start(f32[2,512]{1,0:T(2,128)S(1)} %slice.105), channel_id=1, source_target_pairs={{0,4},{4,8},{8,12},{1,5},{5,9},{9,13},{2,6},{6,10},{10,14},{3,7},{... | collective-permute-start | bytes 12296 | tf_op jit(solution)/shard_map/ppermute | solution.py:12
  278.1 103.2 %copy-start.2 = (bf16[512,512]{1,0:T(8,128)(2,1)S(1)}, bf16[512,512]{1,0:T(8,128)(2,1)}, u32[]{:S(2)}) copy-start(bf16[512,512]{1,0:T(8,128)(2,1)} %param.7) | copy-start | bytes 1572868
  283.0 125.2 %all-gather.21.cloned.1.call-start = ((), (), s32[]{:S(2)}) async-start(), calls=%async_computation.6 | async-start | bytes 2621440 | tf_op jit(solution)/shard_map/all_gather | solution.py:45
  385.5 60.0 %all-gather.23.cloned.1.call-start = ((), (), s32[]{:S(2)}) async-start(), calls=%async_computation.7 | async-start | bytes 2621440 | tf_op jit(solution)/shard_map/all_gather | solution.py:57
  408.3 2.2 copy-start.1
  410.5 3.1 copy-start.8
  413.6 6.1 %copy-start.7 = (bf16[2,2048,512]{2,1,0:T(8,128)(2,1)S(1)}, bf16[2,2048,512]{2,1,0:T(8,128)(2,1)}, u32[]{:S(2)}) copy-start(bf16[2,2048,512]{2,1,0:T(8,128)(2,1)} %all-gather.11.cloned.1.call-done) | copy-start | bytes 12582916
  414.9 4.7 %collective-permute-start.1 = (f32[2,512]{1,0:T(2,128)S(1)}, f32[2,512]{1,0:T(2,128)S(1)}, u32[]{:S(2)}, u32[]{:S(2)}) collective-permute-start(f32[2,512]{1,0:T(2,128)S(1)} %slice.112), channel_id=1, source_target_pairs={{0,4},{4,8},{8,12},{1,5},{5,9},{9,13},{2,6},{6,10},{10,14},{3,7},{... | collective-permute-start | bytes 12296 | tf_op jit(solution)/shard_map/ppermute | solution.py:12
  419.6 25.9 %copy-start.3 = (bf16[512,512]{1,0:T(8,128)(2,1)S(1)}, bf16[512,512]{1,0:T(8,128)(2,1)}, u32[]{:S(2)}) copy-start(bf16[512,512]{1,0:T(8,128)(2,1)} %fusion.31) | copy-start | bytes 1572868
Sparse Core Ops, SparseCore 0:
  8.9 25.2 all-gather.8
  35.8 80.7 all-gather.14
  118.1 79.2 all-gather.12
  198.8 79.2 all-gather.10
  279.5 79.2 all-gather.18
  360.2 21.0 all-gather.16
  385.7 22.5 all-gather.20
  422.1 23.3 all-gather.22
where the time goes:
time: 457 us
  waiting for transfers between devices  408 us (89%)
  matrix products  25.9 us (6%)
  between operations  13.6 us (3%)
  starting transfers between devices  4.96 us (1%)
    all_gather x1, waiting for transfers between devices, shards(): lax.all_gather(value_weight, 'sp', axis=1, tiled=True)  80.1 us
    all_gather x1, waiting for transfers between devices, shards(): lax.all_gather(mix_weight, 'sp', axis=1, tiled=True)  77.9 us
    all_gather x1, waiting for transfers between devices, shards(): lax.all_gather(gate_weight, 'sp', axis=1, tiled=True)  76.4 us
    all_gather x1, waiting for transfers between devices, shards(): lax.all_gather(out_weight, 'sp', axis=1, tiled=True)  75.7 us
    all_gather x2, waiting for transfers between devices, shards(): whole = lax.all_gather(stream, 'tp', axis=1, tiled=True)  46.9 us
    all_gather x2, waiting for transfers between devices, shards(): mixed_all = lax.all_gather(mixed, 'tp', axis=1, tiled=True)  46 us
  transfers between devices with their start and end apart: 10, of which 9 were waited for; matrix products, arithmetic and copies ran while one was open for 3% of the time, Pallas kernels for 0%

commit v1 on v0

--- a/solution.py
+++ b/solution.py
@@ -37,7 +37,9 @@
     stream = tokens
     gathered = (
         lax.all_gather(gate_weight, "sp", axis=1, tiled=True),
-        lax.all_gather(mix_weight, "sp", axis=1, tiled=True),
+        jnp.concatenate(
+            lax.all_to_all(jnp.stack([mix_weight] * lax.axis_size("sp")), "sp", 0, 0), axis=1
+        ),
         lax.all_gather(value_weight, "sp", axis=1, tiled=True),
         lax.all_gather(out_weight, "sp", axis=1, tiled=True),
     )

time: 457 us -> 438 us (0.958)
  waiting for transfers between devices: 408 us -> 379 us
  local copies, waits for them, and re-layouts: 0.05 us -> 7.24 us
  starting transfers between devices: 4.96 us -> 11.4 us
    all_to_all x0 -> x1, waiting for transfers between devices: none -> 142 us  [shards(): lax.all_to_all(jnp.stack([mix_weight] * lax.axis_size('sp')), 'sp', 0, 0)]
    all_gather x1, waiting for transfers between devices: 80.1 us -> 0.02 us  [shards(): lax.all_gather(value_weight, 'sp', axis=1, tiled=True)]
    all_gather x1 -> x0, waiting for transfers between devices: 77.9 us -> none  [shards(): lax.all_gather(mix_weight, 'sp', axis=1, tiled=True)]
    all_gather x2, waiting for transfers between devices: 46.9 us -> 38.7 us  [shards(): whole = lax.all_gather(stream, 'tp', axis=1, tiled=True)]
    all_to_all x0 -> x1, starting transfers between devices: none -> 6.48 us  [shards(): lax.all_to_all(jnp.stack([mix_weight] * lax.axis_size('sp')), 'sp', 0, 0)]
  transfers between devices with their start and end apart: 10 -> 10, of which waited for: 9 -> 8; matrix products, arithmetic and copies ran while one was open for 3% -> 4% of each run, Pallas kernels for 0% -> 0%
where the time goes in v1:
time: 438 us
  waiting for transfers between devices  379 us (87%)
  matrix products  22.7 us (5%)
  between operations  13.6 us (3%)
  starting transfers between devices  11.4 us (3%)
  local copies, waits for them, and re-layouts  7.24 us (2%)
    all_to_all x1, waiting for transfers between devices, shards(): lax.all_to_all(jnp.stack([mix_weight] * lax.axis_size('sp')), 'sp', 0, 0)  142 us
    all_gather x1, waiting for transfers between devices, shards(): lax.all_gather(out_weight, 'sp', axis=1, tiled=True)  75.7 us
    all_gather x1, waiting for transfers between devices, shards(): lax.all_gather(gate_weight, 'sp', axis=1, tiled=True)  72 us
    all_gather x2, waiting for transfers between devices, shards(): mixed_all = lax.all_gather(mixed, 'tp', axis=1, tiled=True)  46 us
    all_gather x2, waiting for transfers between devices, shards(): whole = lax.all_gather(stream, 'tp', axis=1, tiled=True)  38.7 us
  transfers between devices with their start and end apart: 10, of which 8 were waited for; matrix products, arithmetic and copies ran while one was open for 4% of the time, Pallas kernels for 0%

profile of v1, /device:TPU:0, one launch (start us, length us, event | category | flops | bytes accessed | tf_op | source)
XLA Modules:
  0.0 437.9 jit_solution(17798335006289847450)
XLA Ops:
  6.5 0.0 copy-start.3
  6.5 0.0 all-gather.8.cloned.1.call-start
  6.5 0.7 all-gather.8.cloned.1.call-update
  7.3 0.0 all-gather.12.cloned.1.call-start
  7.3 0.7 all-gather.12.cloned.1.call-update
  8.0 0.0 all-gather.10.cloned.1.call-start
  8.1 0.7 all-gather.10.cloned.1.call-update
  8.7 0.0 copy-done.3
  8.8 2.3 stack.2
  11.1 0.0 copy-start.6
  11.1 6.5 %all-to-all-start = ((bf16[4,2,512,512]{3,2,1,0:T(8,128)(2,1)}), bf16[4,2,512,512]{3,2,1,0:T(8,128)(2,1)}, u32[]{:S(2)}, u32[]{:S(2)}) async-start(bf16[4,2,512,512]{3,2,1,0:T(8,128)(2,1)} %stack.2), calls=%async_computation | async-start | bytes 8388608 | tf_op jit(solution)/shard_map/all_to_all | solution.py:41
  17.6 0.0 all-gather.16.cloned.1.call-start
  17.6 0.6 all-gather.16.cloned.1.call-update
  18.1 0.0 all-gather.14.cloned.1.call-start
  18.2 0.0 copy-done.6
  18.2 16.0 %all-gather.8.cloned.1.call-done = bf16[512,2048]{1,0:T(8,128)(2,1)} async-done(((bf16[512,512]{1,0:T(8,128)(2,1)}), bf16[512,2048]{1,0:T(8,128)(2,1)}) %all-gather.8.cloned.1.call-update) | async-done | bytes 2097168 | tf_op jit(solution)/shard_map/all_gather | solution.py:47
  34.2 2.1 fusion
  36.3 142.2 %all-to-all-done = bf16[4,2,512,512]{3,2,1,0:T(8,128)(2,1)} async-done(((bf16[4,2,512,512]{3,2,1,0:T(8,128)(2,1)}), bf16[4,2,512,512]{3,2,1,0:T(8,128)(2,1)}, u32[]{:S(2)}, u32[]{:S(2)}) %all-to-all-start) | async-done | bytes 4194336 | tf_op jit(solution)/shard_map/all_to_all | solution.py:41
  178.5 0.0 copy-start
  178.5 4.0 fusion.52
  182.5 0.0 copy-done
  182.5 1.3 fusion.25
  183.8 0.0 copy-start.7
  183.8 0.0 all-gather.12.cloned.1.call-done
  183.8 2.9 fusion.18
  186.7 0.0 copy-start.8
  186.7 1.3 collective-permute-start
  188.0 0.0 copy-done.8
  188.1 0.0 copy-done.7
  188.1 72.0 %all-gather.10.cloned.1.call-done = bf16[2,2048,512]{2,1,0:T(8,128)(2,1)} async-done(((bf16[2,512,512]{2,1,0:T(8,128)(2,1)}), bf16[2,2048,512]{2,1,0:T(8,128)(2,1)}) %all-gather.10.cloned.1.call-update) | async-done | bytes 4194320 | tf_op jit(solution)/shard_map/all_gather | solution.py:39
  260.1 0.0 collective-permute-done
  260.1 0.0 copy-start.4
  260.1 4.9 %fusion.39 = bf16[512,512]{1,0:T(8,128)(2,1)} fusion(f32[2,512]{1,0:T(2,128)S(1)} %collective-permute-done, f32[512,512]{1,0:T(8,128)} %copy-done.8, f32[512]{0:T(512)S(1)} %bitcast.76, f32[512]{0:T(512)S(1)} %bitcast.77, f32[512]{0:T(512)S(1)} %bitcast.78, bf16[2,2048,512]{2,1,0:T(8,128)(2,1)} %all-gather.10.cloned.1.call-done, ...), kind=kOutput, calls=%fused_computation.55 | convolution fusion | flops 1080819712 | bytes 5787648 | tf_op jit(solution)/shard_map/dot_general | solution.py:49
  265.0 0.0 all-gather.14.cloned.1.call-update
  265.0 0.0 all-gather.18.cloned.1.call-start
  265.1 75.7 %all-gather.16.cloned.1.call-done = bf16[2,2048,512]{2,1,0:T(8,128)(2,1)} async-done(((bf16[2,512,512]{2,1,0:T(8,128)(2,1)}), bf16[2,2048,512]{2,1,0:T(8,128)(2,1)}) %all-gather.16.cloned.1.call-update) | async-done | bytes 4194320 | tf_op jit(solution)/shard_map/all_gather | solution.py:44
  340.8 22.5 %all-gather.14.cloned.1.call-done = bf16[512,2048]{1,0:T(8,128)(2,1)} async-done(((bf16[512,512]{1,0:T(8,128)(2,1)}), bf16[512,2048]{1,0:T(8,128)(2,1)}) %all-gather.14.cloned.1.call-update) | async-done | bytes 2097168 | tf_op jit(solution)/shard_map/all_gather | solution.py:59
  363.3 0.0 copy-done.4
  363.3 0.0 copy-start.2
  363.3 4.4 %fusion.27 = bf16[512,512]{1,0:T(8,128)(2,1)} fusion(bf16[512,2048]{1,0:T(8,128)(2,1)} %all-gather.14.cloned.1.call-done, bf16[2,2048,512]{2,1,0:T(8,128)(2,1)} %all-gather.16.cloned.1.call-done, bf16[512,512]{1,0:T(8,128)(2,1)S(1)} %copy-done.4), kind=kOutput, calls=%fused_computation.39 | convolution fusion | flops 1074528256 | bytes 5242880 | tf_op jit(solution)/shard_map/dot_general | solution.py:60
  367.7 0.0 all-gather.18.cloned.1.call-update
  367.8 0.0 all-gather.20.cloned.1.call-start
  367.8 22.7 %all-gather.18.cloned.1.call-done = bf16[512,2048]{1,0:T(8,128)(2,1)} async-done(((bf16[512,512]{1,0:T(8,128)(2,1)}), bf16[512,2048]{1,0:T(8,128)(2,1)}) %all-gather.18.cloned.1.call-update) | async-done | bytes 2097168 | tf_op jit(solution)/shard_map/all_gather | solution.py:47
  390.5 0.0 copy-start.1
  390.5 2.2 fusion.3
  392.7 0.0 copy-done.2
  392.7 0.0 copy-done.1
  392.7 0.0 copy-start.10
  392.7 1.3 fusion.24
  394.0 0.9 copy-done.10
  394.9 0.0 copy-start.9
  394.9 1.3 fusion.23
  396.3 3.4 collective-permute-start.1
  399.7 1.3 collective-permute-done.1
  401.0 0.0 copy-done.9
  401.0 0.0 copy-start.5
  401.0 2.3 fusion.33
  403.3 0.0 all-gather.20.cloned.1.call-update
  403.3 23.5 %all-gather.20.cloned.1.call-done = bf16[512,2048]{1,0:T(8,128)(2,1)} async-done(((bf16[512,512]{1,0:T(8,128)(2,1)}), bf16[512,2048]{1,0:T(8,128)(2,1)}) %all-gather.20.cloned.1.call-update) | async-done | bytes 2097168 | tf_op jit(solution)/shard_map/all_gather | solution.py:59
  426.8 0.0 copy-done.5
  426.8 4.3 fusion.26
  (6 shorter events, 0.1 us)
Async XLA Ops:
  6.5 2.2 copy-start.3
  6.5 27.7 %all-gather.8.cloned.1.call-start = ((), (), s32[]{:S(2)}) async-start(), calls=%async_computation.1 | async-start | bytes 2621440 | tf_op jit(solution)/shard_map/all_gather | solution.py:47
  7.3 176.6 %all-gather.12.cloned.1.call-start = ((), (), s32[]{:S(2)}) async-start(), calls=%async_computation.3 | async-start | bytes 5242880 | tf_op jit(solution)/shard_map/all_gather | solution.py:43
  8.0 252.1 %all-gather.10.cloned.1.call-start = ((), (), s32[]{:S(2)}) async-start(), calls=%async_computation.2 | async-start | bytes 5242880 | tf_op jit(solution)/shard_map/all_gather | solution.py:39
  11.1 7.1 %copy-start.6 = (bf16[2,2048]{1,0:T(2,128)(2,1)S(1)}, bf16[2,2048]{1,0:T(2,128)(2,1)}, u32[]{:S(2)}) copy-start(bf16[2,2048]{1,0:T(2,128)(2,1)} %param.8) | copy-start | bytes 24580
  11.1 167.4 %all-to-all-start = ((bf16[4,2,512,512]{3,2,1,0:T(8,128)(2,1)}), bf16[4,2,512,512]{3,2,1,0:T(8,128)(2,1)}, u32[]{:S(2)}, u32[]{:S(2)}) async-start(bf16[4,2,512,512]{3,2,1,0:T(8,128)(2,1)} %stack.2), calls=%async_computation | async-start | bytes 8388608 | tf_op jit(solution)/shard_map/all_to_all | solution.py:41
  17.6 323.3 %all-gather.16.cloned.1.call-start = ((), (), s32[]{:S(2)}) async-start(), calls=%async_computation.5 | async-start | bytes 5242880 | tf_op jit(solution)/shard_map/all_gather | solution.py:44
  18.1 345.2 %all-gather.14.cloned.1.call-start = ((), (), s32[]{:S(2)}) async-start(), calls=%async_computation.4 | async-start | bytes 2621440 | tf_op jit(solution)/shard_map/all_gather | solution.py:59
  178.5 4.0 copy-start
  183.8 4.3 copy-start.7
  186.7 1.3 copy-start.8
  186.7 73.4 %collective-permute-start = (f32[2,512]{1,0:T(2,128)S(1)}, f32[2,512]{1,0:T(2,128)S(1)}, u32[]{:S(2)}, u32[]{:S(2)}) collective-permute-start(f32[2,512]{1,0:T(2,128)S(1)} %slice.107), channel_id=1, source_target_pairs={{0,4},{4,8},{8,12},{1,5},{5,9},{9,13},{2,6},{6,10},{10,14},{3,7},{... | collective-permute-start | bytes 12296 | tf_op jit(solution)/shard_map/ppermute | solution.py:12
  260.1 103.2 %copy-start.4 = (bf16[512,512]{1,0:T(8,128)(2,1)S(1)}, bf16[512,512]{1,0:T(8,128)(2,1)}, u32[]{:S(2)}) copy-start(bf16[512,512]{1,0:T(8,128)(2,1)} %param.7) | copy-start | bytes 1572868
  265.0 125.4 %all-gather.18.cloned.1.call-start = ((), (), s32[]{:S(2)}) async-start(), calls=%async_computation.6 | async-start | bytes 2621440 | tf_op jit(solution)/shard_map/all_gather | solution.py:47
  363.3 29.4 %copy-start.2 = (bf16[1,4,512,512]{3,2,0,1:T(8,128)(2,1)S(1)}, bf16[1,4,512,512]{3,2,0,1:T(8,128)(2,1)}, u32[]{:S(2)}) copy-start(bf16[1,4,512,512]{3,2,0,1:T(8,128)(2,1)} %get-tuple-element.6) | copy-start | bytes 6291460
  367.8 59.1 %all-gather.20.cloned.1.call-start = ((), (), s32[]{:S(2)}) async-start(), calls=%async_computation.7 | async-start | bytes 2621440 | tf_op jit(solution)/shard_map/all_gather | solution.py:59
  390.5 2.2 copy-start.1
  392.7 2.2 copy-start.10
  394.9 6.1 %copy-start.9 = (bf16[2,2048,512]{2,1,0:T(8,128)(2,1)S(1)}, bf16[2,2048,512]{2,1,0:T(8,128)(2,1)}, u32[]{:S(2)}) copy-start(bf16[2,2048,512]{2,1,0:T(8,128)(2,1)} %all-gather.10.cloned.1.call-done) | copy-start | bytes 12582916
  396.3 4.7 %collective-permute-start.1 = (f32[2,512]{1,0:T(2,128)S(1)}, f32[2,512]{1,0:T(2,128)S(1)}, u32[]{:S(2)}, u32[]{:S(2)}) collective-permute-start(f32[2,512]{1,0:T(2,128)S(1)} %slice.114), channel_id=1, source_target_pairs={{0,4},{4,8},{8,12},{1,5},{5,9},{9,13},{2,6},{6,10},{10,14},{3,7},{... | collective-permute-start | bytes 12296 | tf_op jit(solution)/shard_map/ppermute | solution.py:12
  401.0 25.8 %copy-start.5 = (bf16[512,512]{1,0:T(8,128)(2,1)S(1)}, bf16[512,512]{1,0:T(8,128)(2,1)}, u32[]{:S(2)}) copy-start(bf16[512,512]{1,0:T(8,128)(2,1)} %fusion.27) | copy-start | bytes 1572868
Sparse Core Ops, SparseCore 0:
  8.9 25.2 all-gather.7
  35.8 136.5 all-gather.11
  173.9 86.1 all-gather.9
  261.6 79.2 all-gather.15
  342.2 21.0 all-gather.13
  367.9 22.5 all-gather.17
  403.4 23.3 all-gather.19
